TPU v7x, 512 devices: a whole 4x8x8 slice. The times are simulated.
512 devices in a mesh: ep: 32 (over z, x), tp: 16 (over y, core).
Axes of the slice: x: 4, y: 8, z: 8, core: 2. Of those that a mesh axis runs over, the one named last changes fastest.
Arguments:
- mixer_rows: bfloat16 [4096, 2048], P('ep'), may hold values from -40 to 40
- mixer_gain: float32 [2048], replicated, may hold values from 0.1 to 1.9
- inner_weight: bfloat16 [2048, 1024], P(None, 'tp'), may hold values from -0.125 to 0.125
- gate_in_weight: bfloat16 [2048, 1024], P(None, 'tp'), may hold values from -0.125 to 0.125
- gate_out_weight: bfloat16 [2048, 1024], P(None, 'tp'), may hold values from -0.125 to 0.125
- conv_taps: float32 [3, 1024], P(None, 'tp'), may hold values from -3.5 to 3.5
- mixer_out_weight: bfloat16 [1024, 2048], P('tp'), may hold values from -0.1875 to 0.1875
- routed_rows: bfloat16 [8192, 2048], P('ep'), may hold values from -40 to 40
- routed_gain: float32 [2048], replicated, may hold values from 0.1 to 1.9
- route_ids: int32 [8192, 2], P('ep'), may hold values from 0 to 31, all different within a row; in each aligned block of 256 rows (0 to 255, 256 to 511, ...) at most 32 rows name the same one
- route_weights: float32 [8192, 2], P('ep'), may hold values from 0.25 to 1
- expert_gate: bfloat16 [32, 2048, 2048], P('ep', None, 'tp'), may hold values from -0.125 to 0.125
- expert_up: bfloat16 [32, 2048, 2048], P('ep', None, 'tp'), may hold values from -0.125 to 0.125
- expert_down: bfloat16 [32, 2048, 2048], P('ep', 'tp'), may hold values from -0.125 to 0.125
Outputs:
- mixer_output: bfloat16 [4096, 2048], P('ep')
- routed_output: bfloat16 [8192, 2048], P('ep')
Inputs may be any that keep to these rules, and one draw needn't show every extreme that they name: `route_ids`: within each aligned block of 256 tokens, no expert is named by more than 32 choices, a bound that some block reaches; a token's 2 experts differ.
All inputs are finite; a program needn't handle non-finite values.
Results may differ from a plain program's by a relative error of at most 0.019.
Values may be sent and summed in bfloat16 or wider, within the bound.
A program may use at most 64 MiB of HBM per device.

v0:
```python
import jax
import jax.numpy as jnp
from jax import lax
from jax.sharding import PartitionSpec as P


def shifted(value, axis, steps):
    count = lax.axis_size(axis)
    initial, last = (max(0, -steps), min(count, count - steps))
    return lax.ppermute(value, axis, [(source, source + steps) for source in range(initial, last)])


def packed_total(arrays, axis):
    ends = [0]
    for a in arrays:
        ends.append(ends[-1] + a.size)
    so_far = lax.psum(jnp.concatenate([a.ravel() for a in arrays]), axis)
    return tuple((so_far[b:e].reshape(a.shape) for a, b, e in zip(arrays, ends, ends[1:])))


def rms_scale(row_block, gain_row):
    values = row_block.astype(jnp.float32)
    scaled = values * lax.rsqrt(jnp.mean(values * values, axis=-1, keepdims=True) + 1e-06)
    return (scaled * gain_row).astype(jnp.bfloat16)


def on_device(
    mixer_rows,
    mixer_gain,
    inner_weight,
    gate_in_weight,
    gate_out_weight,
    conv_taps,
    mixer_out_weight,
    routed_rows,
    routed_gain,
    route_ids,
    route_weights,
    expert_gate,
    expert_up,
    expert_down,
):
    normed = rms_scale(mixer_rows, mixer_gain)
    inner_proj = jnp.dot(normed, inner_weight, preferred_element_type=jnp.float32)
    gate_in = jnp.dot(normed, gate_in_weight, preferred_element_type=jnp.float32)
    conv_input = (gate_in * inner_proj).astype(jnp.bfloat16)
    gate_out = jnp.dot(normed, gate_out_weight, preferred_element_type=jnp.float32)
    tap_total = conv_taps.shape[0]
    rim_rows = tap_total - 1
    earlier_rows = shifted(conv_input[conv_input.shape[0] - rim_rows :], "ep", 1)
    extended = jnp.concatenate([earlier_rows, conv_input], axis=0).astype(jnp.float32)
    length = conv_input.shape[0]
    conv_out = jnp.zeros(conv_input.shape, jnp.float32)
    for tap_index in range(tap_total):
        conv_out = conv_out + conv_taps[tap_index] * extended[tap_index : tap_index + length]
    gated_conv = (gate_out * conv_out).astype(jnp.bfloat16)
    mixer_terms = jnp.dot(gated_conv, mixer_out_weight, preferred_element_type=jnp.float32)
    routed_normed = rms_scale(routed_rows, routed_gain)
    experts = lax.axis_size("ep")
    groups = lax.axis_size("tp")
    column = lax.axis_index("tp")
    tok_count, pick_count = route_ids.shape
    model_width = routed_rows.shape[1]
    capacity = 2 * tok_count * pick_count // experts
    share_rows = capacity // groups
    flat_ids = route_ids.reshape(-1)
    onehot = (flat_ids[:, None] == jnp.arange(experts, dtype=jnp.int32)[None, :]).astype(jnp.int32)
    slot_rank = jnp.sum((jnp.cumsum(onehot, axis=0) - onehot) * onehot, axis=1)
    slot_number = slot_rank * experts + flat_ids
    owners = jnp.arange(tok_count * pick_count, dtype=jnp.int32) // pick_count
    matches = slot_number[None, :] == jnp.arange(capacity * experts, dtype=jnp.int32)[:, None]
    token_table = jnp.where(
        jnp.any(matches, axis=1), jnp.sum(jnp.where(matches, owners[None, :], 0), axis=1), tok_count
    )
    padded_rows = jnp.concatenate(
        [routed_normed, jnp.zeros((1, model_width), jnp.bfloat16)], axis=0
    )
    table_share = lax.dynamic_slice_in_dim(
        token_table.reshape(capacity, experts), column * share_rows, share_rows, 0
    )
    outgoing = jnp.take(padded_rows, table_share.reshape(-1), axis=0).reshape(
        share_rows, experts, model_width
    )
    arrived = lax.all_to_all(outgoing, "ep", split_axis=1, concat_axis=1, tiled=True)
    incoming = lax.all_gather(arrived, "tp", axis=0, tiled=True)
    slot_rows = incoming.reshape(capacity * experts, model_width)
    gate_act = jnp.dot(slot_rows, expert_gate[0], preferred_element_type=jnp.float32)
    up_act = jnp.dot(slot_rows, expert_up[0], preferred_element_type=jnp.float32)
    hidden = (jax.nn.silu(gate_act) * up_act).astype(jnp.bfloat16)
    summed = lax.psum_scatter(
        jnp.dot(hidden, expert_down[0], preferred_element_type=jnp.float32).astype(jnp.bfloat16),
        "tp",
        scatter_dimension=0,
        tiled=True,
    )
    returned = lax.all_to_all(
        summed.reshape(share_rows, experts, model_width),
        "ep",
        split_axis=1,
        concat_axis=1,
        tiled=True,
    )
    flat_back = jnp.concatenate(
        [
            returned.reshape(share_rows * experts, model_width),
            jnp.zeros((1, model_width), jnp.bfloat16),
        ],
        axis=0,
    )
    local_slot = jnp.where(
        slot_rank // share_rows == column,
        (slot_rank - column * share_rows) * experts + flat_ids,
        share_rows * experts,
    )
    contrib = (
        jnp.take(flat_back, local_slot, axis=0).astype(jnp.float32)
        * route_weights.reshape(-1)[:, None]
    )
    routed_terms = jnp.sum(contrib.reshape(tok_count, pick_count, model_width), axis=1)
    mixer_total, routed_total = tuple(
        (
            part.astype(jnp.float32)
            for part in packed_total(
                (mixer_terms.astype(jnp.bfloat16), routed_terms.astype(jnp.bfloat16)), "tp"
            )
        )
    )
    return (mixer_total.astype(jnp.bfloat16), routed_total.astype(jnp.bfloat16))


def solution(mesh):
    return jax.shard_map(
        on_device,
        mesh=mesh,
        in_specs=(
            P("ep", None),
            P(),
            P(None, "tp"),
            P(None, "tp"),
            P(None, "tp"),
            P(None, "tp"),
            P("tp", None),
            P("ep", None),
            P(),
            P("ep", None),
            P("ep", None),
            P("ep", None, "tp"),
            P("ep", None, "tp"),
            P("ep", "tp", None),
        ),
        out_specs=(P("ep", None), P("ep", None)),
        check_vma=False,
    )
```

profile of v0, /device:TPU:1, one launch (start us, length us, event | category | flops | bytes accessed | tf_op | source)
XLA Modules:
  0.0 321.4 jit_solution(4402862292982536007)
XLA Ops:
  7.2 0.9 copy.70
  8.5 1.2 reduce-window.6
  10.8 1.5 fusion
  12.4 1.0 fusion.2
  14.6 24.8 %all_to_all.10 = bf16[2,32,2048]{2,0,1:T(2,128)(2,1)S(1)} all-to-all(bf16[2,32,2048]{2,0,1:T(2,128)(2,1)S(1)} %broadcast_select_fusion.1), channel_id=1, replica_groups=mesh['ep'=32,'tp'=16] {'ep'}, dimensions={1} | all-to-all | bytes 524288 | tf_op jit(solution)/shard_map/all_to_all | solution.py:84
  40.3 42.1 %all-gather.2.cloned.1.call-done = bf16[32,32,2048]{2,1,0:T(8,128)(2,1)} async-done(((bf16[2,32,2048]{2,1,0:T(8,128)(2,1)}), bf16[32,32,2048]{2,1,0:T(8,128)(2,1)}) %all-gather.2.cloned.1.call-update) | async-done | bytes 4194320 | tf_op jit(solution)/shard_map/all_gather | solution.py:85
  82.4 3.5 %fusion.14 = f32[1024,128]{1,0:T(8,128)S(1)} fusion(bf16[1024,2048]{1,0:T(8,128)(2,1)} %bitcast.56, bf16[1,2048,128]{2,1,0:T(8,128)(2,1)S(1)} %copy-done.3), kind=kOutput, calls=%fused_computation.30 | convolution fusion | flops 536870912 | bytes 5242880 | tf_op jit(solution)/shard_map/dot_general | solution.py:87
  86.0 8.5 %convolution_convert_fusion = bf16[1024,2048]{1,0:T(8,128)(2,1)} fusion(bf16[1024,2048]{1,0:T(8,128)(2,1)} %bitcast.57, bf16[1,128,2048]{2,1,0:T(8,128)(2,1)S(1)} %copy-done, bf16[1,2048,128]{2,1,0:T(8,128)(2,1)S(1)} %copy-done.4, f32[1024,128]{1,0:T(8,128)S(1)} %fusion.14), kind=kOutput, calls=%fused_computation.4 | convolution fusion | flops 1076625408 | bytes 9961472 | tf_op jit(solution)/shard_map/dot_general | solution.py:91
  94.5 1.0 copy-done.2
  96.5 3.1 collective-permute-start
  100.1 56.6 %reduce-scatter.2.cloned.1.call-done = bf16[64,2048]{1,0:T(8,128)(2,1)} async-done(((bf16[1024,2048]{1,0:T(8,128)(2,1)}), bf16[64,2048]{1,0:T(8,128)(2,1)}) %reduce-scatter.2.cloned.1.call-update) | async-done | bytes 262160 | tf_op jit(solution)/shard_map/reduce_scatter | solution.py:90
  156.7 1.9 copy.82
  158.6 9.1 %all-to-all-start.1 = ((bf16[2,32,2048]{2,0,1:T(2,128)(2,1)}), bf16[2,32,2048]{2,0,1:T(2,128)(2,1)S(1)}, u32[]{:S(2)}, u32[]{:S(2)}) async-start(bf16[2,32,2048]{2,0,1:T(2,128)(2,1)} %copy.82), calls=%async_computation.2 | async-start | bytes 524288 | tf_op jit(solution)/shard_map/all_to_all | solution.py:96
  168.1 0.8 copy.85
  169.0 0.9 fusion.4
  170.1 8.1 %all-to-all-done.1 = bf16[2,32,2048]{2,0,1:T(2,128)(2,1)S(1)} async-done(((bf16[2,32,2048]{2,0,1:T(2,128)(2,1)}), bf16[2,32,2048]{2,0,1:T(2,128)(2,1)S(1)}, u32[]{:S(2)}, u32[]{:S(2)}) %all-to-all-start.1) | async-done | bytes 262176 | tf_op jit(solution)/shard_map/all_to_all | solution.py:96
  178.3 2.5 gather_fusion.1
  180.8 2.7 gather.15
  183.4 9.9 %multiply_reduce_fusion = bf16[256,2048]{1,0:T(8,128)(2,1)S(1)} fusion(bf16[256,2,2048]{2,1,0:T(2,128)(2,1)} %gather.15, pred[256,2]{1,0:T(8,128)(4,1)S(1)} %copy.78, f32[256,2]{1,0:T(8,128)S(1)} %copy-done.5), kind=kLoop, calls=%fused_computation.2 | loop fusion | flops 3670016 | bytes 3148288 | tf_op jit(solution)/shard_map/reduce_sum | solution.py:119
  193.5 1.3 pad_maximum_fusion
  194.8 116.5 %all-reduce.4.cloned.1.call-done = bf16[786432]{0:T(1024)(128)(2,1)} async-done(((bf16[786432]{0:T(1024)(128)(2,1)}), bf16[786432]{0:T(1024)(128)(2,1)}) %all-reduce.4.cloned.1.call-update) | async-done | bytes 1572880 | tf_op jit(solution)/shard_map/psum | solution.py:17
  311.4 1.2 slice-done
  312.6 1.3 slice.65
  313.8 1.0 slice.63
  (77 shorter events, 6.0 us)
Async XLA Ops:
  7.2 78.8 %copy-start = (bf16[1,128,2048]{2,1,0:T(8,128)(2,1)S(1)}, bf16[1,128,2048]{2,1,0:T(8,128)(2,1)}, u32[]{:S(2)}) copy-start(bf16[1,128,2048]{2,1,0:T(8,128)(2,1)} %param.27) | copy-start | bytes 1572868
  7.2 5.3 %copy-start.1 = (bf16[256,2048]{1,0:T(8,128)(2,1)S(1)}, bf16[256,2048]{1,0:T(8,128)(2,1)}, u32[]{:S(2)}) copy-start(bf16[256,2048]{1,0:T(8,128)(2,1)} %param.21) | copy-start | bytes 3145732
  7.2 75.2 %all-gather.2.cloned.1.call-start = ((), (), s32[]{:S(2)}) async-start(), calls=%async_computation.3 | async-start | bytes 4456448 | tf_op jit(solution)/shard_map/all_gather | solution.py:85
  13.5 68.9 %copy-start.3 = (bf16[1,2048,128]{2,1,0:T(8,128)(2,1)S(1)}, bf16[1,2048,128]{2,1,0:T(8,128)(2,1)}, u32[]{:S(2)}) copy-start(bf16[1,2048,128]{2,1,0:T(8,128)(2,1)} %param.25) | copy-start | bytes 1572868
  40.3 116.4 %reduce-scatter.2.cloned.1.call-start = ((), (), s32[]{:S(2)}) async-start(), calls=%async_computation.4 | async-start | bytes 4456448 | tf_op jit(solution)/shard_map/reduce_scatter | solution.py:90
  82.4 3.5 %copy-start.4 = (bf16[1,2048,128]{2,1,0:T(8,128)(2,1)S(1)}, bf16[1,2048,128]{2,1,0:T(8,128)(2,1)}, u32[]{:S(2)}) copy-start(bf16[1,2048,128]{2,1,0:T(8,128)(2,1)} %param.26) | copy-start | bytes 1572868
  94.4 1.0 copy-start.2
  94.4 1.3 copy-start.8
  94.4 1.3 copy-start.12
  94.4 1.7 copy-start.13
  95.5 4.5 %copy-start.9 = (s32[256,2]{0,1:T(2,128)S(1)}, s32[256,2]{0,1:T(2,128)}, u32[]{:S(2)}) copy-start(s32[256,2]{0,1:T(2,128)} %param.23) | copy-start | bytes 6148
  95.5 72.4 %copy-start.11 = (f32[3,64]{1,0:T(4,128)S(1)}, f32[3,64]{1,0:T(4,128)}, u32[]{:S(2)}) copy-start(f32[3,64]{1,0:T(4,128)} %param.19) | copy-start | bytes 2308
  95.5 72.7 %copy-start.10 = (f32[256,2]{0,1:T(2,128)S(1)}, f32[256,2]{0,1:T(2,128)}, u32[]{:S(2)}) copy-start(f32[256,2]{0,1:T(2,128)} %param.24) | copy-start | bytes 6148
  95.7 73.4 %copy-start.6 = (bf16[64,2048]{1,0:T(8,128)(2,1)S(1)}, bf16[64,2048]{1,0:T(8,128)(2,1)}, u32[]{:S(2)}) copy-start(bf16[64,2048]{1,0:T(8,128)(2,1)} %param.20) | copy-start | bytes 786436
  95.7 73.4 %copy-start.7 = (bf16[2048,64]{0,1:T(8,128)(2,1)S(1)}, bf16[2048,64]{0,1:T(8,128)(2,1)}, u32[]{:S(2)}) copy-start(bf16[2048,64]{0,1:T(8,128)(2,1)} %param.18) | copy-start | bytes 786436
  96.5 72.4 %collective-permute-start = (bf16[2,64]{0,1:T(8,128)(2,1)S(1)}, bf16[2,64]{0,1:T(8,128)(2,1)S(1)}, u32[]{:S(2)}, u32[]{:S(2)}) collective-permute-start(bf16[2,64]{0,1:T(8,128)(2,1)S(1)} %slice.70), channel_id=1, source_target_pairs={{0,16},{16,32},{32,48},{48,64},{64,80},{80,96},{96,112},{112,128},... | collective-permute-start | bytes 776 | tf_op jit(solution)/shard_map/ppermute | solution.py:10
  158.6 19.6 %all-to-all-start.1 = ((bf16[2,32,2048]{2,0,1:T(2,128)(2,1)}), bf16[2,32,2048]{2,0,1:T(2,128)(2,1)S(1)}, u32[]{:S(2)}, u32[]{:S(2)}) async-start(bf16[2,32,2048]{2,0,1:T(2,128)(2,1)} %copy.82), calls=%async_computation.2 | async-start | bytes 524288 | tf_op jit(solution)/shard_map/all_to_all | solution.py:96
  167.7 143.7 %all-reduce.4.cloned.1.call-start = ((), (), s32[]{:S(2)}) async-start(), calls=%async_computation.5 | async-start | bytes 3145728 | tf_op jit(solution)/shard_map/psum | solution.py:17
  180.8 2.7 copy-start.5
  311.3 1.2 slice-start
  312.6 1.3 slice-start.1
Sparse Core Ops, SparseCore 0:
  40.4 42.0 all-gather.1
  94.6 62.0 reduce-scatter.1
  194.9 116.3 all-reduce.3
where the time goes:
time: 322 us; the launch traced here: 321 us
  waiting for transfers between devices  223 us (69%)
  blocking collectives  24.8 us (8%)
  local copies, waits for them, and re-layouts  16.8 us (5%)
  other arithmetic  16.3 us (5%)
  between operations  14.1 us (4%)
  matrix products  13.6 us (4%)
  starting transfers between devices  12.5 us (4%)
    psum x1, waiting for transfers between devices, packed_total(): so_far = lax.psum(jnp.concatenate([a.ravel() for a in arrays]), axis)  117 us
    reduce_scatter x1, waiting for transfers between devices, on_device(): lax.psum_scatter(jnp.dot(hidden, expert_down[0], preferred_element_type=j...  56.6 us
    all_gather x1, waiting for transfers between devices, on_device(): incoming = lax.all_gather(arrived, 'tp', axis=0, tiled=True)  42.1 us
    all_to_all x1, blocking collectives, on_device(): lax.all_to_all(outgoing, 'ep', split_axis=1, concat_axis=1, tiled=True)  24.8 us
    reduce_sum x1, other arithmetic, on_device(): jnp.sum(contrib.reshape(tok_count, pick_count, model_width), axis=1)  9.87 us
    all_to_all x1, starting transfers between devices, on_device(): lax.all_to_all(summed.reshape(share_rows, experts, model_width), 'ep', sp...  9.09 us
    dot_general x1, matrix products, on_device(): jnp.dot(hidden, expert_down[0], preferred_element_type=jnp.float32)  8.47 us
    all_to_all x1, waiting for transfers between devices, on_device(): lax.all_to_all(summed.reshape(share_rows, experts, model_width), 'ep', sp...  8.08 us
  transfers between devices with their start and end apart: 5, of which 4 were waited for; matrix products, arithmetic and copies ran while one was open for 2% of the time, Pallas kernels for 0%

commit v1 on v0

--- a/solution.py
+++ b/solution.py
@@ -14,7 +14,12 @@
     ends = [0]
     for a in arrays:
         ends.append(ends[-1] + a.size)
-    so_far = lax.psum(jnp.concatenate([a.ravel() for a in arrays]), axis)
+
+    def measure_hubs_now(my_tile, dev_axis):
+        tmp = lax.all_gather(my_tile, axis_name=dev_axis)
+        return jnp.sum(tmp, axis=0)
+
+    so_far = measure_hubs_now(jnp.concatenate([a.ravel() for a in arrays]), axis)
     return tuple((so_far[b:e].reshape(a.shape) for a, b, e in zip(arrays, ends, ends[1:])))
 
 

time: 322 us -> 402 us (1.25)
  other arithmetic: 16.3 us -> 49.1 us
  local copies, waits for them, and re-layouts: 16.8 us -> 44.5 us
  waiting for transfers between devices: 223 us -> 243 us
    all_gather x0 -> x1, waiting for transfers between devices: none -> 135 us  [measure_hubs_now(): tmp = lax.all_gather(my_tile, axis_name=dev_axis)]
    psum x1 -> x0, waiting for transfers between devices: 117 us -> none  [packed_total(): so_far = lax.psum(jnp.concatenate([a.ravel() for a in arrays]), axis)]
    reduce_sum x0 -> x1, other arithmetic: none -> 32.8 us  [measure_hubs_now(): return jnp.sum(tmp, axis=0)]
    all_gather x0 -> x1, local copies, waits for them, and re-layouts: none -> 28.7 us  [measure_hubs_now(): tmp = lax.all_gather(my_tile, axis_name=dev_axis)]
  transfers between devices with their start and end apart: 5 -> 5, of which waited for: 4 -> 4; matrix products, arithmetic and copies ran while one was open for 2% -> 1% of each run, Pallas kernels for 0% -> 0%
where the time goes in v1:
time: 402 us; the launch traced here: 401 us
  waiting for transfers between devices  243 us (60%)
  other arithmetic  49.1 us (12%)
  local copies, waits for them, and re-layouts  44.5 us (11%)
  blocking collectives  24.8 us (6%)
  between operations  14.1 us (4%)
  matrix products  13.6 us (3%)
  starting transfers between devices  12.1 us (3%)
    all_gather x1, waiting for transfers between devices, measure_hubs_now(): tmp = lax.all_gather(my_tile, axis_name=dev_axis)  135 us
    reduce_scatter x1, waiting for transfers between devices, on_device(): lax.psum_scatter(jnp.dot(hidden, expert_down[0], preferred_element_type=j...  56.8 us
    all_gather x1, waiting for transfers between devices, on_device(): incoming = lax.all_gather(arrived, 'tp', axis=0, tiled=True)  42.1 us
    reduce_sum x1, other arithmetic, measure_hubs_now(): return jnp.sum(tmp, axis=0)  32.8 us
    all_gather x1, local copies, waits for them, and re-layouts, measure_hubs_now(): tmp = lax.all_gather(my_tile, axis_name=dev_axis)  28.7 us
    all_to_all x1, blocking collectives, on_device(): lax.all_to_all(outgoing, 'ep', split_axis=1, concat_axis=1, tiled=True)  24.8 us
    reduce_sum x1, other arithmetic, on_device(): jnp.sum(contrib.reshape(tok_count, pick_count, model_width), axis=1)  9.87 us
    all_to_all x1, waiting for transfers between devices, on_device(): lax.all_to_all(summed.reshape(share_rows, experts, model_width), 'ep', sp...  8.73 us
  transfers between devices with their start and end apart: 5, of which 4 were waited for; matrix products, arithmetic and copies ran while one was open for 1% of the time, Pallas kernels for 0%

profile of v1, /device:TPU:1, one launch (start us, length us, event | category | flops | bytes accessed | tf_op | source)
XLA Modules:
  0.0 401.4 jit_solution(1957484743586592318)
XLA Ops:
  7.2 0.9 copy.70
  8.5 1.5 fusion
  10.0 1.2 reduce-window.6
  12.4 1.0 fusion.2
  14.6 24.8 %all_to_all.10 = bf16[2,32,2048]{2,0,1:T(2,128)(2,1)S(1)} all-to-all(bf16[2,32,2048]{2,0,1:T(2,128)(2,1)S(1)} %broadcast_select_fusion.1), channel_id=1, replica_groups=mesh['ep'=32,'tp'=16] {'ep'}, dimensions={1} | all-to-all | bytes 524288 | tf_op jit(solution)/shard_map/all_to_all | solution.py:89
  40.3 42.1 %all-gather.4.cloned.1.call-done = bf16[32,32,2048]{2,1,0:T(8,128)(2,1)} async-done(((bf16[2,32,2048]{2,1,0:T(8,128)(2,1)}), bf16[32,32,2048]{2,1,0:T(8,128)(2,1)}) %all-gather.4.cloned.1.call-update) | async-done | bytes 4194320 | tf_op jit(solution)/shard_map/all_gather | solution.py:90
  82.4 3.5 fusion.14
  86.0 8.5 %convolution_convert_fusion = bf16[1024,2048]{1,0:T(8,128)(2,1)} fusion(bf16[1024,2048]{1,0:T(8,128)(2,1)} %bitcast.57, bf16[1,128,2048]{2,1,0:T(8,128)(2,1)S(1)} %copy-done, bf16[1,2048,128]{2,1,0:T(8,128)(2,1)S(1)} %copy-done.6, f32[1024,128]{1,0:T(8,128)S(1)} %fusion.14), kind=kOutput, calls=%fused_computation.4 | convolution fusion | flops 1076625408 | bytes 9961472 | tf_op jit(solution)/shard_map/dot_general | solution.py:96
  94.4 1.0 copy-done.3
  96.5 3.1 collective-permute-start
  100.1 56.8 %reduce-scatter.2.cloned.1.call-done = bf16[64,2048]{1,0:T(8,128)(2,1)} async-done(((bf16[1024,2048]{1,0:T(8,128)(2,1)}), bf16[64,2048]{1,0:T(8,128)(2,1)}) %reduce-scatter.2.cloned.1.call-update) | async-done | bytes 262160 | tf_op jit(solution)/shard_map/reduce_scatter | solution.py:95
  156.8 1.9 copy.82
  158.8 8.7 %all-to-all-start.1 = ((bf16[2,32,2048]{2,0,1:T(2,128)(2,1)}), bf16[2,32,2048]{2,0,1:T(2,128)(2,1)S(1)}, u32[]{:S(2)}, u32[]{:S(2)}) async-start(bf16[2,32,2048]{2,0,1:T(2,128)(2,1)} %copy.82), calls=%async_computation.2 | async-start | bytes 524288 | tf_op jit(solution)/shard_map/all_to_all | solution.py:101
  168.2 0.9 fusion.4
  169.3 8.7 %all-to-all-done.1 = bf16[2,32,2048]{2,0,1:T(2,128)(2,1)S(1)} async-done(((bf16[2,32,2048]{2,0,1:T(2,128)(2,1)}), bf16[2,32,2048]{2,0,1:T(2,128)(2,1)S(1)}, u32[]{:S(2)}, u32[]{:S(2)}) %all-to-all-start.1) | async-done | bytes 262176 | tf_op jit(solution)/shard_map/all_to_all | solution.py:101
  178.1 2.5 gather_fusion.1
  180.6 2.7 gather.15
  183.2 9.9 %multiply_reduce_fusion = bf16[256,2048]{1,0:T(8,128)(2,1)S(1)} fusion(bf16[256,2,2048]{2,1,0:T(2,128)(2,1)} %gather.15, pred[256,2]{1,0:T(8,128)(4,1)S(1)} %copy.78, f32[256,2]{1,0:T(8,128)S(1)} %copy.85), kind=kLoop, calls=%fused_computation.2 | loop fusion | flops 3670016 | bytes 3148288 | tf_op jit(solution)/shard_map/reduce_sum | solution.py:124
  193.3 1.3 pad_maximum_fusion
  194.7 135.4 %all-gather.6.cloned.1.call-done = bf16[12582912]{0:T(1024)(128)(2,1)} async-done(((bf16[786432]{0:T(1024)(128)(2,1)}), bf16[12582912]{0:T(1024)(128)(2,1)}) %all-gather.6.cloned.1.call-update) | async-done | bytes 25165840 | tf_op jit(solution)/shard_map/all_gather | solution.py:19
  330.1 28.7 %reshape.267 = bf16[16,786432]{1,0:T(8,128)(2,1)} reshape(bf16[12582912]{0:T(1024)(128)(2,1)} %all-gather.6.cloned.1.call-done) | data formatting | bytes 50331648 | tf_op jit(solution)/shard_map/all_gather | solution.py:19
  358.8 32.8 %reduce_sum.68 = bf16[786432]{0:T(1024)(128)(2,1)S(1)} reduce(bf16[16,786432]{1,0:T(8,128)(2,1)} %reshape.267, bf16[]{:T(256)} %constant.82.clone.1), dimensions={0}, to_apply=%region_9.10 | reduce | flops 11796480 | bytes 26738690 | tf_op jit(solution)/shard_map/reduce_sum | solution.py:20
  392.6 1.3 slice.65
  393.8 1.0 slice.63
  (79 shorter events, 7.1 us)
Async XLA Ops:
  7.2 78.8 %copy-start = (bf16[1,128,2048]{2,1,0:T(8,128)(2,1)S(1)}, bf16[1,128,2048]{2,1,0:T(8,128)(2,1)}, u32[]{:S(2)}) copy-start(bf16[1,128,2048]{2,1,0:T(8,128)(2,1)} %param.27) | copy-start | bytes 1572868
  7.2 5.3 %copy-start.2 = (bf16[256,2048]{1,0:T(8,128)(2,1)S(1)}, bf16[256,2048]{1,0:T(8,128)(2,1)}, u32[]{:S(2)}) copy-start(bf16[256,2048]{1,0:T(8,128)(2,1)} %param.21) | copy-start | bytes 3145732
  7.2 75.2 %all-gather.4.cloned.1.call-start = ((), (), s32[]{:S(2)}) async-start(), calls=%async_computation.3 | async-start | bytes 4456448 | tf_op jit(solution)/shard_map/all_gather | solution.py:90
  13.5 68.9 %copy-start.5 = (bf16[1,2048,128]{2,1,0:T(8,128)(2,1)S(1)}, bf16[1,2048,128]{2,1,0:T(8,128)(2,1)}, u32[]{:S(2)}) copy-start(bf16[1,2048,128]{2,1,0:T(8,128)(2,1)} %param.25) | copy-start | bytes 1572868
  40.3 116.6 %reduce-scatter.2.cloned.1.call-start = ((), (), s32[]{:S(2)}) async-start(), calls=%async_computation.4 | async-start | bytes 4456448 | tf_op jit(solution)/shard_map/reduce_scatter | solution.py:95
  82.4 3.5 copy-start.6
  94.4 1.0 copy-start.3
  94.4 1.3 copy-start.9
  94.4 1.3 copy-start.13
  94.4 1.7 copy-start.14
  95.5 4.5 %copy-start.10 = (s32[256,2]{0,1:T(2,128)S(1)}, s32[256,2]{0,1:T(2,128)}, u32[]{:S(2)}) copy-start(s32[256,2]{0,1:T(2,128)} %param.23) | copy-start | bytes 6148
  95.5 72.3 %copy-start.12 = (f32[3,64]{1,0:T(4,128)S(1)}, f32[3,64]{1,0:T(4,128)}, u32[]{:S(2)}) copy-start(f32[3,64]{1,0:T(4,128)} %param.19) | copy-start | bytes 2308
  95.5 72.5 %copy-start.11 = (f32[256,2]{0,1:T(2,128)S(1)}, f32[256,2]{0,1:T(2,128)}, u32[]{:S(2)}) copy-start(f32[256,2]{0,1:T(2,128)} %param.24) | copy-start | bytes 6148
  95.6 72.5 %copy-start.7 = (bf16[64,2048]{1,0:T(8,128)(2,1)S(1)}, bf16[64,2048]{1,0:T(8,128)(2,1)}, u32[]{:S(2)}) copy-start(bf16[64,2048]{1,0:T(8,128)(2,1)} %param.20) | copy-start | bytes 786436
  95.7 72.5 %copy-start.8 = (bf16[2048,64]{0,1:T(8,128)(2,1)S(1)}, bf16[2048,64]{0,1:T(8,128)(2,1)}, u32[]{:S(2)}) copy-start(bf16[2048,64]{0,1:T(8,128)(2,1)} %param.18) | copy-start | bytes 786436
  96.5 71.6 %collective-permute-start = (bf16[2,64]{0,1:T(8,128)(2,1)S(1)}, bf16[2,64]{0,1:T(8,128)(2,1)S(1)}, u32[]{:S(2)}, u32[]{:S(2)}) collective-permute-start(bf16[2,64]{0,1:T(8,128)(2,1)S(1)} %slice.70), channel_id=1, source_target_pairs={{0,16},{16,32},{32,48},{48,64},{64,80},{80,96},{96,112},{112,128},... | collective-permute-start | bytes 776 | tf_op jit(solution)/shard_map/ppermute | solution.py:10
  158.8 19.2 %all-to-all-start.1 = ((bf16[2,32,2048]{2,0,1:T(2,128)(2,1)}), bf16[2,32,2048]{2,0,1:T(2,128)(2,1)S(1)}, u32[]{:S(2)}, u32[]{:S(2)}) async-start(bf16[2,32,2048]{2,0,1:T(2,128)(2,1)} %copy.82), calls=%async_computation.2 | async-start | bytes 524288 | tf_op jit(solution)/shard_map/all_to_all | solution.py:101
  167.5 162.6 %all-gather.6.cloned.1.call-start = ((), (), s32[]{:S(2)}) async-start(), calls=%async_computation.5 | async-start | bytes 26738688 | tf_op jit(solution)/shard_map/all_gather | solution.py:19
  392.5 2.4 copy-start.1
  392.5 1.3 copy-start.4
Sparse Core Ops, SparseCore 0:
  40.4 42.0 all-gather.3
  94.6 62.2 reduce-scatter.1
  194.8 135.2 all-gather.5
